TPU v7x, 32 devices: a whole 2x2x4 slice. The times are simulated.
32 devices in a mesh: sp: 8 (over z, y), tp: 4 (over x, core).
Axes of the slice: x: 2, y: 2, z: 4, core: 2. Of those that a mesh axis runs over, the one named last changes fastest.
Arguments:
- tokens: bfloat16 [3072, 2048], P(('sp', 'tp')), may hold values from -6 to 6
- input_norm_gain: bfloat16 [2048], replicated, may hold values from 0.099609375 to 1.8984375
- output_gate_weight: bfloat16 [2048, 2048], P('sp', 'tp'), may hold values from -0.125 to 0.125
- value_input_weight: bfloat16 [2048, 2048], P('sp', 'tp'), may hold values from -0.125 to 0.125
- recurrence_input_weight: bfloat16 [2048, 2048], P('sp', 'tp'), may hold values from -0.125 to 0.125
- convolution_filter: bfloat16 [3, 2048], P(None, 'tp'), may hold values from -3.5 to 3.5
- recurrence_filter: bfloat16 [4, 2048], P(None, 'tp'), may hold values from -3 to 3
- recurrence_gate_matrix: bfloat16 [8, 256, 256], P('tp'), may hold values from -0.375 to 0.375
- input_gate_matrix: bfloat16 [8, 256, 256], P('tp'), may hold values from -0.375 to 0.375
- channel_decay_rate: float32 [2048], P('tp'), may hold values from 1.6276042e-05 to 0.025
- head_log_decay_add: float32 [8, 3072], P('tp', 'sp'), may hold values from -0.7 to 0
- initial_state: float32 [2048], P('tp'), may hold values from -6 to 6
- output_matrix: bfloat16 [2048, 2048], P(None, 'tp'), may hold values from -0.125 to 0.125
Outputs:
- mixed: bfloat16 [3072, 2048], P(('sp', 'tp'))
All inputs are finite; a program needn't handle non-finite values.
Results may differ from a plain program's by a relative error of at most 0.015.
Values may be sent and summed in bfloat16 or wider, within the bound.
A program may use at most 64 MiB of HBM per device.

v0:
```python
import jax
import jax.numpy as jnp
from jax import lax
from jax.sharding import PartitionSpec as P

DECAY_MULTIPLIER = 8.0
NORM_EPS = 1e-06


def shifted(value, axis, steps):
    count = lax.axis_size(axis)
    first, last = (max(0, -steps), min(count, count - steps))
    return lax.ppermute(value, axis, [(source, source + steps) for source in range(first, last)])


def causal_taps(values, before, tap_weights):
    extended = jnp.concatenate([before, values], axis=0).astype(jnp.float32)
    length = values.shape[0]
    summed = jnp.zeros((length, values.shape[1]), jnp.float32)
    for offset in range(tap_weights.shape[0]):
        summed = (
            summed + tap_weights[offset].astype(jnp.float32) * extended[offset : offset + length]
        )
    return summed


def linear_step(first_pair, second_pair):
    return (first_pair[0] * second_pair[0], second_pair[0] * first_pair[1] + second_pair[1])


def shards(
    tokens,
    input_norm_gain,
    output_gate_weight,
    value_input_weight,
    recurrence_input_weight,
    convolution_filter,
    recurrence_filter,
    recurrence_gate_matrix,
    input_gate_matrix,
    channel_decay_rate,
    head_log_decay_add,
    initial_state,
    output_matrix,
):
    token_rows = tokens.astype(jnp.float32)
    inverse_rms = lax.rsqrt(jnp.mean(token_rows * token_rows, axis=1, keepdims=True) + NORM_EPS)
    normed = (token_rows * inverse_rms * input_norm_gain.astype(jnp.float32)).astype(jnp.bfloat16)
    channel_count = output_gate_weight.shape[1]
    weights = (
        lax.all_gather(output_gate_weight, "sp", axis=0, tiled=True),
        lax.all_gather(value_input_weight, "sp", axis=0, tiled=True),
        lax.all_gather(recurrence_input_weight, "sp", axis=0, tiled=True),
    )
    row_block = lax.all_gather(normed, "tp", axis=0, tiled=True)
    projected = jnp.concatenate(
        [
            jnp.dot(row_block, weight, preferred_element_type=jnp.float32).astype(jnp.bfloat16)
            for weight in weights
        ],
        axis=1,
    )
    gate_proj = projected[:, :channel_count]
    value_proj = projected[:, channel_count : 2 * channel_count]
    recur_proj = projected[:, 2 * channel_count :]
    value_tail, recur_tail = shifted(
        (
            value_proj[-(convolution_filter.shape[0] - 1) :],
            recur_proj[-(recurrence_filter.shape[0] - 1) :],
        ),
        "sp",
        1,
    )
    conv_mix = gate_proj.astype(jnp.float32) * causal_taps(
        value_proj, value_tail, convolution_filter
    )
    recur_in = causal_taps(recur_proj, recur_tail, recurrence_filter).astype(jnp.bfloat16)
    length = recur_in.shape[0]
    number_of_heads = recurrence_gate_matrix.shape[0]
    head_width = channel_count // number_of_heads
    grouped = recur_in.reshape(length, number_of_heads, head_width)
    forget_gate = jax.nn.sigmoid(
        jnp.einsum(
            "thi,hij->thj", grouped, recurrence_gate_matrix, preferred_element_type=jnp.float32
        ).reshape(length, channel_count)
    )
    admit_gate = jax.nn.sigmoid(
        jnp.einsum(
            "thi,hij->thj", grouped, input_gate_matrix, preferred_element_type=jnp.float32
        ).reshape(length, channel_count)
    )
    decay_add_rows = jnp.repeat(head_log_decay_add.T, head_width, axis=1)
    logarithm_decay = -DECAY_MULTIPLIER * forget_gate * channel_decay_rate[None, :] + decay_add_rows
    decay_step = jnp.exp(logarithm_decay)
    drive_term = (
        recur_in.astype(jnp.float32) * admit_gate * jnp.sqrt(-jnp.expm1(2.0 * logarithm_decay))
    )
    cum_decay, local_state = lax.associative_scan(linear_step, (decay_step, drive_term), axis=0)
    block_log = jnp.sum(logarithm_decay, axis=0)
    block_end = local_state[-1]
    all_logs, all_ends = (
        lax.all_gather(block_log[None, :], "sp", axis=0, tiled=True),
        lax.all_gather(block_end[None, :], "sp", axis=0, tiled=True),
    )
    devices = all_logs.shape[0]
    position = lax.axis_index("sp")
    earlier = (jnp.arange(devices, dtype=jnp.int32) < position)[:, None]
    masked_logs = jnp.where(earlier, all_logs, 0.0)
    through = jnp.cumsum(masked_logs, axis=0)
    prior_log = jnp.sum(masked_logs, axis=0)
    weights_back = jnp.where(earlier, jnp.exp(jnp.minimum(prior_log[None, :] - through, 0.0)), 0.0)
    incoming = jnp.exp(prior_log) * initial_state + jnp.sum(weights_back * all_ends, axis=0)
    hidden = local_state + cum_decay * incoming[None, :]
    merged = (conv_mix + hidden).astype(jnp.bfloat16)
    contract = (((1,), (1,)), ((), ()))
    return lax.psum_scatter(
        lax.dot_general(merged, output_matrix, contract, preferred_element_type=jnp.float32).astype(
            jnp.bfloat16
        ),
        "tp",
        scatter_dimension=0,
        tiled=True,
    )


def solution(mesh):
    placed = (
        P(("sp", "tp"), None),
        P(),
        P("sp", "tp"),
        P("sp", "tp"),
        P("sp", "tp"),
        P(None, "tp"),
        P(None, "tp"),
        P("tp", None, None),
        P("tp", None, None),
        P("tp"),
        P("tp", "sp"),
        P("tp"),
        P(None, "tp"),
    )
    return jax.shard_map(
        shards, mesh=mesh, in_specs=placed, out_specs=P(("sp", "tp"), None), check_vma=False
    )
```

profile of v0, /device:TPU:0, one launch (start us, length us, event | category | flops | bytes accessed | tf_op | source)
XLA Modules:
  0.0 281.9 jit_solution(6480056698027380360)
XLA Ops:
  8.6 1.9 fusion.12
  14.0 19.0 %all-gather.7.cloned.1.call-done = bf16[384,2048]{1,0:T(8,128)(2,1)} async-done(((bf16[96,2048]{1,0:T(8,128)(2,1)}), bf16[384,2048]{1,0:T(8,128)(2,1)}) %all-gather.7.cloned.1.call-update) | async-done | bytes 1572880 | tf_op jit(solution)/shard_map/all_gather | solution.py:55
  33.1 51.2 %all-gather.11.cloned.1.call-done = bf16[2048,512]{1,0:T(8,128)(2,1)} async-done(((bf16[256,512]{1,0:T(8,128)(2,1)}), bf16[2048,512]{1,0:T(8,128)(2,1)}) %all-gather.11.cloned.1.call-update) | async-done | bytes 2097168 | tf_op jit(solution)/shard_map/all_gather | solution.py:52
  84.3 3.0 %convolution_convert_fusion.2 = bf16[384,512]{1,0:T(8,128)(2,1)S(1)} fusion(bf16[384,2048]{1,0:T(8,128)(2,1)} %all-gather.7.cloned.1.call-done, bf16[2048,512]{1,0:T(8,128)(2,1)} %all-gather.11.cloned.1.call-done), kind=kOutput, calls=%fused_computation.10 | convolution fusion | flops 805502976 | bytes 4063232 | tf_op jit(solution)/shard_map/dot_general | solution.py:58
  87.4 2.5 collective-permute-start
  89.8 44.3 %all-gather.13.cloned.1.call-done = bf16[2048,512]{1,0:T(8,128)(2,1)} async-done(((bf16[256,512]{1,0:T(8,128)(2,1)}), bf16[2048,512]{1,0:T(8,128)(2,1)}) %all-gather.13.cloned.1.call-update) | async-done | bytes 2097168 | tf_op jit(solution)/shard_map/all_gather | solution.py:53
  134.1 3.0 %convolution_convert_fusion.1 = bf16[384,512]{1,0:T(8,128)(2,1)S(1)} fusion(bf16[384,2048]{1,0:T(8,128)(2,1)} %all-gather.7.cloned.1.call-done, bf16[2048,512]{1,0:T(8,128)(2,1)} %all-gather.13.cloned.1.call-done), kind=kOutput, calls=%fused_computation.9 | convolution fusion | flops 805502976 | bytes 4063232 | tf_op jit(solution)/shard_map/dot_general | solution.py:58
  137.1 2.5 collective-permute-start.1
  142.9 2.3 copy.30
  145.2 2.3 fusion.22
  147.5 2.3 copy.31
  149.8 3.4 %sqrt_multiply_fusion = (f32[384,512]{1,0:T(8,128)S(1)}, f32[384,512]{1,0:T(8,128)}) fusion(f32[384,512]{1,0:T(8,128)} %copy.30, f32[384,512]{1,0:T(8,128)} %copy.32, f32[384,512]{1,0:T(8,128)} %copy.31, f32[512]{0:T(512)S(1)} %broadcast_multiply_fusion, f32[387,512]{1,0:T(8,128)S(1)} %maximum_convert_fusion.1, f32[512]{0:T(512)S(1)} %bitcast.56, ...), kind=kLoop, calls=%fused_computation.41 | loop fusion | flops 2949120 | bytes 7088128 | tf_op jit(solution)/shard_map/mul | solution.py:96
  154.2 3.2 %slice.363 = f32[191,512]{1,0:T(8,128)} slice(f32[384,512]{1,0:T(8,128)} %copy-done.2), slice={[2:384:2], [0:512:1]} | slice | bytes 782336 | tf_op jit(solution)/shard_map/slice | solution.py:98
  157.3 2.1 slice.307
  159.4 3.2 %slice.306 = f32[192,512]{1,0:T(8,128)} slice(f32[384,512]{1,0:T(8,128)} %copy-done.2), slice={[0:383:2], [0:512:1]} | slice | bytes 786432 | tf_op jit(solution)/shard_map/slice | solution.py:98
  172.1 27.3 %all-gather = f32[8,1,512]{2,1,0:T(1,128)S(1)} all-gather(f32[1,1,512]{2,1,0:T(1,128)S(1)} %reshape.51), channel_id=1, replica_groups=mesh['sp'=8,'tp'=4] {'sp'}, dimensions={0}, use_global_device_ids=true | all-gather | bytes 18432 | tf_op jit(solution)/shard_map/all_gather | solution.py:102
  203.1 2.5 pad.127
  205.6 1.9 add.261
  209.4 1.9 pad.112
  211.3 2.9 %pad.113 = f32[384,512]{1,0:T(8,128)} pad(f32[192,512]{1,0:T(8,128)} %add.252, f32[]{:T(128)} %constant.8.clone.1), padding=1_0_1x0_0_0 | pad | bytes 1179652 | tf_op jit(solution)/shard_map/pad | solution.py:98
  214.3 2.0 pad.128
  217.1 26.1 %all-gather.1 = f32[8,1,512]{2,1,0:T(1,128)S(1)} all-gather(f32[1,1,512]{2,1,0:T(1,128)S(1)} %add_bitcast_fusion), channel_id=1, replica_groups=mesh['sp'=8,'tp'=4] {'sp'}, dimensions={0}, use_global_device_ids=true | all-gather | bytes 18432 | tf_op jit(solution)/shard_map/all_gather | solution.py:103
  243.3 6.7 %convolution_convert_fusion = bf16[384,2048]{1,0:T(8,128)(2,1)} fusion(bf16[2048,512]{1,0:T(8,128)(2,1)S(1)} %copy-done, bf16[384,2048]{1,0:T(8,128)(2,1)} %all-gather.7.cloned.1.call-done, bf16[2048,512]{1,0:T(8,128)(2,1)} %all-gather.9.cloned.1.call-done, f32[386,512]{1,0:T(8,128)} %maximum_convert_fusion, f32[384,512]{1,0:T(8,128)} %pad.128, ...), kind=kOutput, calls=%fused_computation | convolution fusion | flops 1614151680 | bytes 12853248 | tf_op jit(solution)/shard_map/dot_general | solution.py:117
  250.1 25.3 %reduce-scatter.2.cloned.1.call-done = bf16[96,2048]{1,0:T(8,128)(2,1)} async-done(((bf16[384,2048]{1,0:T(8,128)(2,1)}), bf16[96,2048]{1,0:T(8,128)(2,1)}) %reduce-scatter.2.cloned.1.call-update) | async-done | bytes 393232 | tf_op jit(solution)/shard_map/reduce_scatter | solution.py:116
  (184 shorter events, 25.2 us)
Async XLA Ops:
  6.5 236.8 %copy-start = (bf16[2048,512]{1,0:T(8,128)(2,1)S(1)}, bf16[2048,512]{1,0:T(8,128)(2,1)}, u32[]{:S(2)}) copy-start(bf16[2048,512]{1,0:T(8,128)(2,1)} %param.25) | copy-start | bytes 6291460
  6.5 6.1 %copy-start.11 = (f32[512]{0:T(512)S(1)}, f32[512]{0:T(512)}, u32[]{:S(2)}) copy-start(f32[512]{0:T(512)} %param.22) | copy-start | bytes 6148
  6.5 6.2 %copy-start.9 = (bf16[3,512]{1,0:T(4,128)(2,1)S(1)}, bf16[3,512]{1,0:T(4,128)(2,1)}, u32[]{:S(2)}) copy-start(bf16[3,512]{1,0:T(4,128)(2,1)} %param.18) | copy-start | bytes 9220
  6.5 6.2 %copy-start.8 = (bf16[4,512]{1,0:T(4,128)(2,1)S(1)}, bf16[4,512]{1,0:T(4,128)(2,1)}, u32[]{:S(2)}) copy-start(bf16[4,512]{1,0:T(4,128)(2,1)} %param.19) | copy-start | bytes 12292
  6.5 6.2 %copy-start.10 = (f32[2,384]{1,0:T(2,128)S(1)}, f32[2,384]{1,0:T(2,128)}, u32[]{:S(2)}) copy-start(f32[2,384]{1,0:T(2,128)} %param.23) | copy-start | bytes 9220
  6.5 26.5 %all-gather.7.cloned.1.call-start = ((), (), s32[]{:S(2)}) async-start(), calls=%async_computation.1 | async-start | bytes 1966080 | tf_op jit(solution)/shard_map/all_gather | solution.py:55
  10.5 73.8 %all-gather.11.cloned.1.call-start = ((), (), s32[]{:S(2)}) async-start(), calls=%async_computation.3 | async-start | bytes 2359296 | tf_op jit(solution)/shard_map/all_gather | solution.py:52
  11.3 122.8 %all-gather.13.cloned.1.call-start = ((), (), s32[]{:S(2)}) async-start(), calls=%async_computation.4 | async-start | bytes 2359296 | tf_op jit(solution)/shard_map/all_gather | solution.py:53
  12.0 231.3 %all-gather.9.cloned.1.call-start = ((), (), s32[]{:S(2)}) async-start(), calls=%async_computation.2 | async-start | bytes 2359296 | tf_op jit(solution)/shard_map/all_gather | solution.py:51
  12.6 262.8 %reduce-scatter.2.cloned.1.call-start = ((), (), s32[]{:S(2)}) async-start(), calls=%async_computation.5 | async-start | bytes 1966080 | tf_op jit(solution)/shard_map/reduce_scatter | solution.py:116
  87.4 52.3 %collective-permute-start = (bf16[2,512]{1,0:T(2,128)(2,1)S(1)}, bf16[2,512]{1,0:T(2,128)(2,1)S(1)}, u32[]{:S(2)}, u32[]{:S(2)}) collective-permute-start(bf16[2,512]{1,0:T(2,128)(2,1)S(1)} %slice.380), channel_id=1, source_target_pairs={{0,4},{4,8},{8,12},{12,16},{16,20},{20,24},{24,28},{1,5},{5,9},{9,... | collective-permute-start | bytes 6152 | tf_op jit(solution)/shard_map/ppermute | solution.py:13
  137.1 3.8 %collective-permute-start.1 = (bf16[3,512]{1,0:T(4,128)(2,1)S(1)}, bf16[3,512]{1,0:T(4,128)(2,1)S(1)}, u32[]{:S(2)}, u32[]{:S(2)}) collective-permute-start(bf16[3,512]{1,0:T(4,128)(2,1)S(1)} %slice.384), channel_id=1, source_target_pairs={{0,4},{4,8},{8,12},{12,16},{16,20},{20,24},{24,28},{1,5},{5,9},{9,... | collective-permute-start | bytes 9224 | tf_op jit(solution)/shard_map/ppermute | solution.py:13
  140.6 1.0 copy-start.13
  153.2 0.9 copy-start.2
  153.2 9.4 %copy-start.1 = (f32[384,512]{1,0:T(8,128)S(1)}, f32[384,512]{1,0:T(8,128)}, u32[]{:S(2)}) copy-start(f32[384,512]{1,0:T(8,128)} %get-tuple-element.12) | copy-start | bytes 2359300
  205.6 2.7 copy-start.3
  205.6 2.7 copy-start.4
  205.6 2.7 copy-start.5
  209.4 4.9 %copy-start.6 = (f32[191,512]{1,0:T(8,128)S(1)}, f32[191,512]{1,0:T(8,128)}, u32[]{:S(2)}) copy-start(f32[191,512]{1,0:T(8,128)} %get-tuple-element.14) | copy-start | bytes 1173508
  209.4 6.8 %copy-start.7 = (f32[192,512]{1,0:T(8,128)S(1)}, f32[192,512]{1,0:T(8,128)}, u32[]{:S(2)}) copy-start(f32[192,512]{1,0:T(8,128)} %add.261) | copy-start | bytes 1179652
  211.3 32.0 %copy-start.12 = (f32[512]{0:T(512)S(1)}, f32[512]{0:T(512)}, u32[]{:S(2)}) copy-start(f32[512]{0:T(512)} %param.24) | copy-start | bytes 6148
Sparse Core Ops, SparseCore 0:
  10.7 22.3 all-gather.6
  35.2 49.0 all-gather.10
  86.4 47.6 all-gather.12
  136.1 47.7 all-gather.8
  250.2 25.1 reduce-scatter.1
where the time goes:
time: 283 us; the launch traced here: 282 us
  waiting for transfers between devices  142 us (50%)
  blocking collectives  53.4 us (19%)
  local copies, waits for them, and re-layouts  33 us (12%)
  other arithmetic  17.9 us (6%)
  matrix products  16.4 us (6%)
  between operations  14 us (5%)
  starting transfers between devices  5.12 us (2%)
    all_gather x1, waiting for transfers between devices, shards(): lax.all_gather(value_input_weight, 'sp', axis=0, tiled=True)  51.2 us
    all_gather x1, waiting for transfers between devices, shards(): lax.all_gather(recurrence_input_weight, 'sp', axis=0, tiled=True)  44.3 us
    all_gather x1, blocking collectives, shards(): lax.all_gather(block_log[None, :], 'sp', axis=0, tiled=True)  27.3 us
    all_gather x1, blocking collectives, shards(): lax.all_gather(block_end[None, :], 'sp', axis=0, tiled=True)  26.1 us
    reduce_scatter x1, waiting for transfers between devices, shards(): lax.psum_scatter(lax.dot_general(merged, output_matrix, contract, preferr...  25.3 us
    all_gather x1, waiting for transfers between devices, shards(): row_block = lax.all_gather(normed, 'tp', axis=0, tiled=True)  19 us
    slice x56, local copies, waits for them, and re-layouts, shards(): lax.associative_scan(linear_step, (decay_step, drive_term), axis=0)  15.2 us
    pad x30, local copies, waits for them, and re-layouts, shards(): lax.associative_scan(linear_step, (decay_step, drive_term), axis=0)  10.8 us
  transfers between devices with their start and end apart: 7, of which 5 were waited for; matrix products, arithmetic and copies ran while one was open for 20% of the time, Pallas kernels for 0%

commit v1 on v0

--- a/solution.py
+++ b/solution.py
@@ -52,7 +52,12 @@
         lax.all_gather(value_input_weight, "sp", axis=0, tiled=True),
         lax.all_gather(recurrence_input_weight, "sp", axis=0, tiled=True),
     )
-    row_block = lax.all_gather(normed, "tp", axis=0, tiled=True)
+    ring = [normed]
+    for hop in range(3):
+        ring.append(lax.ppermute(ring[-1], "tp", [(dev, (dev + 1) % 4) for dev in range(4)]))
+    row_block = jnp.roll(
+        jnp.concatenate(ring[::-1], axis=0), (lax.axis_index("tp") + 1) * ring[0].shape[0], axis=0
+    )
     projected = jnp.concatenate(
         [
             jnp.dot(row_block, weight, preferred_element_type=jnp.float32).astype(jnp.bfloat16)

time: 283 us -> 338 us (1.19)
  local copies, waits for them, and re-layouts: 33 us -> 99.9 us
  waiting for transfers between devices: 142 us -> 107 us
  other arithmetic: 17.9 us -> 38.7 us
    slice x56, local copies, waits for them, and re-layouts: 15.2 us -> 70.1 us  [shards(): lax.associative_scan(linear_step, (decay_step, drive_term), axis=0)]
    all_gather x1, waiting for transfers between devices: 51.2 us -> 16.7 us  [shards(): lax.all_gather(value_input_weight, 'sp', axis=0, tiled=True)]
    all_gather x1 -> x0, waiting for transfers between devices: 19 us -> none  [shards(): row_block = lax.all_gather(normed, 'tp', axis=0, tiled=True)]
    ppermute x0 -> x3, waiting for transfers between devices: none -> 18.5 us  [shards(): lax.ppermute(ring[-1], 'tp', [(dev, (dev + 1) % 4) for dev in range(4)])]
    add x15, other arithmetic: 3.68 us -> 16.3 us  [linear_step(): second_pair[0] * first_pair[1] + second_pair[1]]
    unnamed x29 -> x57, local copies, waits for them, and re-layouts: 1.16 us -> 8.76 us
    concatenate x15, other arithmetic: 0.23 us -> 5.51 us  [shards(): lax.associative_scan(linear_step, (decay_step, drive_term), axis=0)]
    pad x30, local copies, waits for them, and re-layouts: 10.8 us -> 14.4 us  [shards(): lax.associative_scan(linear_step, (decay_step, drive_term), axis=0)]
  transfers between devices with their start and end apart: 7 -> 9, of which waited for: 5 -> 7; matrix products, arithmetic and copies ran while one was open for 20% -> 44% of each run, Pallas kernels for 0% -> 0%
where the time goes in v1:
time: 338 us; the launch traced here: 335 us
  waiting for transfers between devices  107 us (32%)
  local copies, waits for them, and re-layouts  99.9 us (30%)
  blocking collectives  53.4 us (16%)
  other arithmetic  38.7 us (11%)
  matrix products  17.2 us (5%)
  between operations  13.8 us (4%)
  starting transfers between devices  5.73 us (2%)
    slice x56, local copies, waits for them, and re-layouts, shards(): lax.associative_scan(linear_step, (decay_step, drive_term), axis=0)  70.1 us
    all_gather x1, waiting for transfers between devices, shards(): lax.all_gather(recurrence_input_weight, 'sp', axis=0, tiled=True)  44.2 us
    all_gather x1, blocking collectives, shards(): lax.all_gather(block_log[None, :], 'sp', axis=0, tiled=True)  27.3 us
    all_gather x1, blocking collectives, shards(): lax.all_gather(block_end[None, :], 'sp', axis=0, tiled=True)  26.1 us
    reduce_scatter x1, waiting for transfers between devices, shards(): lax.psum_scatter(lax.dot_general(merged, output_matrix, contract, preferr...  25.3 us
    ppermute x3, waiting for transfers between devices, shards(): lax.ppermute(ring[-1], 'tp', [(dev, (dev + 1) % 4) for dev in range(4)])  18.5 us
    all_gather x1, waiting for transfers between devices, shards(): lax.all_gather(value_input_weight, 'sp', axis=0, tiled=True)  16.7 us
    add x15, other arithmetic, linear_step(): second_pair[0] * first_pair[1] + second_pair[1]  16.3 us
  transfers between devices with their start and end apart: 9, of which 7 were waited for; matrix products, arithmetic and copies ran while one was open for 44% of the time, Pallas kernels for 0%

profile of v1, /device:TPU:0, one launch (start us, length us, event | category | flops | bytes accessed | tf_op | source)
XLA Modules:
  0.0 335.2 jit_solution(9580102540912084040)
XLA Ops:
  11.7 7.5 %collective-permute-done = bf16[96,2048]{1,0:T(8,128)(2,1)} collective-permute-done((bf16[96,2048]{1,0:T(8,128)(2,1)S(1)}, bf16[96,2048]{1,0:T(8,128)(2,1)}, u32[]{:S(2)}, u32[]{:S(2)}) %collective-permute-start) | collective-permute-done | bytes 393248 | tf_op jit(solution)/shard_map/ppermute | solution.py:57
  22.4 4.3 %collective-permute-done.1 = bf16[96,2048]{1,0:T(8,128)(2,1)} collective-permute-done((bf16[96,2048]{1,0:T(8,128)(2,1)}, bf16[96,2048]{1,0:T(8,128)(2,1)}, u32[]{:S(2)}, u32[]{:S(2)}) %collective-permute-start.1) | collective-permute-done | bytes 393248 | tf_op jit(solution)/shard_map/ppermute | solution.py:57
  27.3 6.8 %collective-permute-done.2 = bf16[96,2048]{1,0:T(8,128)(2,1)S(1)} collective-permute-done((bf16[96,2048]{1,0:T(8,128)(2,1)}, bf16[96,2048]{1,0:T(8,128)(2,1)S(1)}, u32[]{:S(2)}, u32[]{:S(2)}) %collective-permute-start.2) | collective-permute-done | bytes 393248 | tf_op jit(solution)/shard_map/ppermute | solution.py:57
  44.6 16.7 %all-gather.8.cloned.1.call-done = bf16[2048,512]{1,0:T(8,128)(2,1)} async-done(((bf16[256,512]{1,0:T(8,128)(2,1)}), bf16[2048,512]{1,0:T(8,128)(2,1)}) %all-gather.8.cloned.1.call-update) | async-done | bytes 2097168 | tf_op jit(solution)/shard_map/all_gather | solution.py:52
  61.3 3.1 convolution_convert_fusion.2
  64.4 2.5 collective-permute-start.3
  66.9 44.2 %all-gather.10.cloned.1.call-done = bf16[2048,512]{1,0:T(8,128)(2,1)} async-done(((bf16[256,512]{1,0:T(8,128)(2,1)}), bf16[2048,512]{1,0:T(8,128)(2,1)}) %all-gather.10.cloned.1.call-update) | async-done | bytes 2097168 | tf_op jit(solution)/shard_map/all_gather | solution.py:53
  111.1 3.1 convolution_convert_fusion.1
  114.2 2.6 collective-permute-start.4
  120.5 2.3 copy.31
  122.8 2.3 fusion.5
  125.0 2.3 copy.30
  127.4 3.7 %sqrt_multiply_fusion = (f32[384,512]{1,0:T(8,128)}, f32[384,512]{1,0:T(8,128)}) fusion(f32[384,512]{1,0:T(8,128)} %copy.30, f32[384,512]{1,0:T(8,128)} %copy.32, f32[384,512]{1,0:T(8,128)} %copy.31, f32[512]{0:T(512)S(1)} %broadcast_multiply_fusion, f32[387,512]{1,0:T(8,128)S(1)} %maximum_convert_fusion.1, f32[512]{0:T(512)S(1)} %bitcast.53, ...), kind=kLoop, calls=%fused_computation.44 | loop fusion | flops 2949120 | bytes 7088128 | tf_op jit(solution)/shard_map/mul | solution.py:101
  133.2 3.2 slice.307
  136.4 3.2 slice.305
  139.5 3.1 slice.309
  205.6 3.2 slice.363
  228.6 2.5 pad.127
  232.9 2.2 fusion.34
  237.1 27.3 %all-gather = f32[8,1,512]{2,1,0:T(1,128)S(1)} all-gather(f32[1,1,512]{2,1,0:T(1,128)S(1)} %reshape.51), channel_id=1, replica_groups=mesh['sp'=8,'tp'=4] {'sp'}, dimensions={0}, use_global_device_ids=true | all-gather | bytes 18432 | tf_op jit(solution)/shard_map/all_gather | solution.py:107
  264.5 2.9 pad.129
  270.1 26.1 %all-gather.1 = f32[8,1,512]{2,1,0:T(1,128)S(1)} all-gather(f32[1,1,512]{2,1,0:T(1,128)S(1)} %add_bitcast_fusion), channel_id=1, replica_groups=mesh['sp'=8,'tp'=4] {'sp'}, dimensions={0}, use_global_device_ids=true | all-gather | bytes 18432 | tf_op jit(solution)/shard_map/all_gather | solution.py:108
  296.4 7.0 %convolution_convert_fusion = bf16[384,2048]{1,0:T(8,128)(2,1)} fusion(bf16[2048,512]{1,0:T(8,128)(2,1)S(1)} %copy-done, bf16[2048,512]{1,0:T(8,128)(2,1)} %all-gather.6.cloned.1.call-done, bf16[768,2048]{1,0:T(8,128)(2,1)} %constant_dynamic-update-slice_fusion, s32[]{:T(128)S(6)} %select_n.21, f32[386,512]{1,0:T(8,128)} %maximum_convert_fusion, ...), kind=kOutput, calls=%fused_computation | convolution fusion | flops 1614151680 | bytes 12853252 | tf_op jit(solution)/shard_map/dot_general | solution.py:122
  303.4 25.3 %reduce-scatter.2.cloned.1.call-done = bf16[96,2048]{1,0:T(8,128)(2,1)} async-done(((bf16[384,2048]{1,0:T(8,128)(2,1)}), bf16[96,2048]{1,0:T(8,128)(2,1)}) %reduce-scatter.2.cloned.1.call-update) | async-done | bytes 393232 | tf_op jit(solution)/shard_map/reduce_scatter | solution.py:121
  (217 shorter events, 114.2 us)
Async XLA Ops:
  6.5 289.8 %copy-start = (bf16[2048,512]{1,0:T(8,128)(2,1)S(1)}, bf16[2048,512]{1,0:T(8,128)(2,1)}, u32[]{:S(2)}) copy-start(bf16[2048,512]{1,0:T(8,128)(2,1)} %param.25) | copy-start | bytes 6291460
  6.5 20.2 %copy-start.10 = (bf16[3,512]{1,0:T(4,128)(2,1)S(1)}, bf16[3,512]{1,0:T(4,128)(2,1)}, u32[]{:S(2)}) copy-start(bf16[3,512]{1,0:T(4,128)(2,1)} %param.18) | copy-start | bytes 9220
  6.5 20.8 %copy-start.9 = (bf16[4,512]{1,0:T(4,128)(2,1)S(1)}, bf16[4,512]{1,0:T(4,128)(2,1)}, u32[]{:S(2)}) copy-start(bf16[4,512]{1,0:T(4,128)(2,1)} %param.19) | copy-start | bytes 12292
  6.5 54.8 %all-gather.8.cloned.1.call-start = ((), (), s32[]{:S(2)}) async-start(), calls=%async_computation.2 | async-start | bytes 2359296 | tf_op jit(solution)/shard_map/all_gather | solution.py:52
  7.3 103.8 %all-gather.10.cloned.1.call-start = ((), (), s32[]{:S(2)}) async-start(), calls=%async_computation.3 | async-start | bytes 2359296 | tf_op jit(solution)/shard_map/all_gather | solution.py:53
  8.0 30.4 %copy-start.1 = (bf16[96,2048]{1,0:T(8,128)(2,1)S(1)}, bf16[96,2048]{1,0:T(8,128)(2,1)}, u32[]{:S(2)}) copy-start(bf16[96,2048]{1,0:T(8,128)(2,1)} %param.13) | copy-start | bytes 1179652
  8.0 288.3 %all-gather.6.cloned.1.call-start = ((), (), s32[]{:S(2)}) async-start(), calls=%async_computation.1 | async-start | bytes 2359296 | tf_op jit(solution)/shard_map/all_gather | solution.py:51
  11.2 8.0 %collective-permute-start = (bf16[96,2048]{1,0:T(8,128)(2,1)S(1)}, bf16[96,2048]{1,0:T(8,128)(2,1)}, u32[]{:S(2)}, u32[]{:S(2)}) collective-permute-start(bf16[96,2048]{1,0:T(8,128)(2,1)S(1)} %fusion.17), channel_id=1, source_target_pairs={{0,1},{1,2},{2,3},{3,0},{4,5},{5,6},{6,7},{7,4},{8,9},{9,10},{10,1... | collective-permute-start | bytes 1179656 | tf_op jit(solution)/shard_map/ppermute | solution.py:57
  19.2 7.5 %collective-permute-start.1 = (bf16[96,2048]{1,0:T(8,128)(2,1)}, bf16[96,2048]{1,0:T(8,128)(2,1)}, u32[]{:S(2)}, u32[]{:S(2)}) collective-permute-start(bf16[96,2048]{1,0:T(8,128)(2,1)} %collective-permute-done), channel_id=1, source_target_pairs={{0,1},{1,2},{2,3},{3,0},{4,5},{5,6},{6,7},{7,4},{8,9},{9,10},{10,1... | collective-permute-start | bytes 1179656 | tf_op jit(solution)/shard_map/ppermute | solution.py:57
  19.2 309.5 %reduce-scatter.2.cloned.1.call-start = ((), (), s32[]{:S(2)}) async-start(), calls=%async_computation.4 | async-start | bytes 1966080 | tf_op jit(solution)/shard_map/reduce_scatter | solution.py:121
  26.7 7.4 %collective-permute-start.2 = (bf16[96,2048]{1,0:T(8,128)(2,1)}, bf16[96,2048]{1,0:T(8,128)(2,1)S(1)}, u32[]{:S(2)}, u32[]{:S(2)}) collective-permute-start(bf16[96,2048]{1,0:T(8,128)(2,1)} %collective-permute-done.1), channel_id=1, source_target_pairs={{0,1},{1,2},{2,3},{3,0},{4,5},{5,6},{6,7},{7,4},{8,9},{9,10},{10,1... | collective-permute-start | bytes 1179656 | tf_op jit(solution)/shard_map/ppermute | solution.py:57
  64.4 52.4 %collective-permute-start.3 = (bf16[2,512]{1,0:T(2,128)(2,1)S(1)}, bf16[2,512]{1,0:T(2,128)(2,1)S(1)}, u32[]{:S(2)}, u32[]{:S(2)}) collective-permute-start(bf16[2,512]{1,0:T(2,128)(2,1)S(1)} %slice.380), channel_id=1, source_target_pairs={{0,4},{4,8},{8,12},{12,16},{16,20},{20,24},{24,28},{1,5},{5,9},{9,... | collective-permute-start | bytes 6152 | tf_op jit(solution)/shard_map/ppermute | solution.py:13
  114.2 3.9 %collective-permute-start.4 = (bf16[3,512]{1,0:T(4,128)(2,1)S(1)}, bf16[3,512]{1,0:T(4,128)(2,1)S(1)}, u32[]{:S(2)}, u32[]{:S(2)}) collective-permute-start(bf16[3,512]{1,0:T(4,128)(2,1)S(1)} %slice.384), channel_id=1, source_target_pairs={{0,4},{4,8},{8,12},{12,16},{16,20},{20,24},{24,28},{1,5},{5,9},{9,... | collective-permute-start | bytes 9224 | tf_op jit(solution)/shard_map/ppermute | solution.py:13
  145.6 58.5 %copy-start.2 = (f32[384,512]{1,0:T(8,128)S(1)}, f32[384,512]{1,0:T(8,128)}, u32[]{:S(2)}) copy-start(f32[384,512]{1,0:T(8,128)} %get-tuple-element.12) | copy-start | bytes 2359300
  204.1 12.7 %copy-start.16 = (f32[1,512]{1,0:T(1,128)S(1)}, f32[1,512]{1,0:T(1,128)}, u32[]{:S(2)}) copy-start(f32[1,512]{1,0:T(1,128)} %slice.393) | copy-start | bytes 6148
  210.6 9.1 %copy-start.7 = (f32[47,512]{1,0:T(8,128)S(1)}, f32[47,512]{1,0:T(8,128)}, u32[]{:S(2)}) copy-start(f32[47,512]{1,0:T(8,128)} %slice.316) | copy-start | bytes 288772
  210.6 9.1 %copy-start.8 = (f32[47,512]{1,0:T(8,128)S(1)}, f32[47,512]{1,0:T(8,128)}, u32[]{:S(2)}) copy-start(f32[47,512]{1,0:T(8,128)} %slice.359) | copy-start | bytes 288772
  231.1 33.3 %copy-start.18 = (pred[8]{0:T(512)(128)(4,1)S(1)}, pred[8]{0:T(512)(128)(4,1)}, u32[]{:S(2)}) copy-start(pred[8]{0:T(512)(128)(4,1)} %iota_compare_fusion) | copy-start | bytes 28
  232.9 34.5 %copy-start.11 = (f32[1,512]{1,0:T(1,128)S(1)}, f32[1,512]{1,0:T(1,128)}, u32[]{:S(2)}) copy-start(f32[1,512]{1,0:T(1,128)} %slice.415) | copy-start | bytes 6148
  235.1 32.3 %copy-start.4 = (f32[191,512]{1,0:T(8,128)S(1)}, f32[191,512]{1,0:T(8,128)}, u32[]{:S(2)}) copy-start(f32[191,512]{1,0:T(8,128)} %get-tuple-element.14) | copy-start | bytes 1173508
  235.1 61.1 %copy-start.20 = (f32[512]{0:T(512)S(1)}, f32[512]{0:T(512)}, u32[]{:S(2)}) copy-start(f32[512]{0:T(512)} %param.24) | copy-start | bytes 6148
  235.1 61.2 %copy-start.21 = (f32[1,512]{1,0:T(1,128)S(1)}, f32[1,512]{1,0:T(1,128)}, u32[]{:S(2)}) copy-start(f32[1,512]{1,0:T(1,128)} %get-tuple-element.43) | copy-start | bytes 6148
  235.1 61.2 %copy-start.22 = (f32[1,512]{1,0:T(1,128)S(1)}, f32[1,512]{1,0:T(1,128)}, u32[]{:S(2)}) copy-start(f32[1,512]{1,0:T(1,128)} %get-tuple-element.44) | copy-start | bytes 6148
  235.1 61.2 %copy-start.23 = (f32[1,512]{1,0:T(1,128)S(1)}, f32[1,512]{1,0:T(1,128)}, u32[]{:S(2)}) copy-start(f32[1,512]{1,0:T(1,128)} %get-tuple-element.45) | copy-start | bytes 6148
  (10 other events, 49.4 us)
Sparse Core Ops, SparseCore 0:
  9.5 51.7 all-gather.7
  63.4 47.6 all-gather.9
  113.2 47.6 all-gather.5
  303.5 25.1 reduce-scatter.1
